TPU v7x, 32 devices: a whole 2x2x4 slice. The times are simulated.
32 devices in a mesh: sp: 4 (over z), fs: 4 (over y, x), tp: 2 (over core).
Axes of the slice: x: 2, y: 2, z: 4, core: 2. Of those that a mesh axis runs over, the one named last changes fastest.
Arguments:
- tokens: bfloat16 [4, 4096, 2048], P('fs', ('sp', 'tp')), may hold values from -6 to 6
- norm_gain: bfloat16 [2048], replicated, may hold values from 0.099609375 to 1.8984375
- w_query: bfloat16 [2048, 1024], P(None, 'tp'), may hold values from -0.125 to 0.125
- w_key: bfloat16 [2048, 1024], P(None, 'tp'), may hold values from -0.125 to 0.125
- w_value: bfloat16 [2048, 1024], P(None, 'tp'), may hold values from -0.125 to 0.125
- w_outgate: bfloat16 [2048, 1024], P(None, 'tp'), may hold values from -0.125 to 0.125
- w_gatein: bfloat16 [2048, 1024], P(None, 'tp'), may hold values from -0.125 to 0.125
- w_gateout: bfloat16 [2048, 1024], P(None, 'tp'), may hold values from -0.125 to 0.125
- w_convin: bfloat16 [2048, 1024], P(None, 'tp'), may hold values from -0.125 to 0.125
- w_igate: bfloat16 [2048, 8], replicated, may hold values from -0.125 to 0.125
- w_fgate: bfloat16 [2048, 8], replicated, may hold values from -0.125 to 0.125
- input_bias: float32 [8], replicated, may hold values from -1 to 101
- forget_bias: float32 [8], replicated
- forget_extra: float32 [4, 4096, 8], P('fs', 'sp', 'tp'), may hold values from -0.7 to 0
- init_memory: float32 [4, 8, 128, 128], P('fs', 'tp'), may hold values from -56 to 56
- head_gain: bfloat16 [1024], replicated, may hold values from 0.099609375 to 1.8984375
- conv_taps: bfloat16 [3, 1024], replicated, may hold values from -3.5 to 3.5
- out_memory: bfloat16 [1024, 2048], P('tp'), may hold values from -0.125 to 0.125
- out_conv: bfloat16 [1024, 2048], P('tp'), may hold values from -0.125 to 0.125
Outputs:
- layer_out: bfloat16 [4, 4096, 2048], P('fs', ('sp', 'tp'))
All inputs are finite; a program needn't handle non-finite values.
Results may differ from a plain program's by a relative error of at most 0.017.
Values may be sent and summed in bfloat16 or wider, within the bound.
A program may use at most 128 MiB of HBM per device.

v0:
```python
import functools

import jax
import jax.numpy as jnp
from jax import lax
from jax.experimental import pallas as pl
from jax.experimental.pallas import tpu as pltpu
from jax.sharding import PartitionSpec as P

BLOCK = 128
EPSILON = 1e-06
LOWEST_LOG = -1e30
MESH = pl.DeviceIdType.MESH
F32 = jnp.float32
BF16 = jnp.bfloat16
PAD = 8
RIM = 16
NORM_ROWS = 64

KEY, VALUE, GATE_IN, CONV_IN, GATE_OUT, QUERY, OUT_GATE = range(7)


def kernel(
    n_sp,
    tokens,
    norm_gain,
    w_key,
    w_value,
    w_gatein,
    w_convin,
    w_gateout,
    w_query,
    w_outgate,
    w_igate,
    w_fgate,
    input_bias,
    forget_bias,
    extra,
    init_memory,
    head_gain,
    conv_taps,
    out_memory,
    out_conv,
    layer_out,
    tok,
    gain_row,
    head_rows,
    gate_w,
    normed,
    weights,
    out_w,
    proj,
    gate_pre,
    row_log,
    col_log,
    block_sum,
    block_peak,
    terms,
    running,
    running_log,
    starts,
    starts_log,
    seg_memory,
    seg_log,
    got_memory,
    got_log,
    conv_rows,
    rim,
    mix,
    part_send,
    part_got,
    local_sem,
    weight_sem,
    token_sem,
    seg_send,
    seg_recv,
    rim_sem,
    part_sem_send,
    part_sem_recv,
):
    me = lax.axis_index("tp")
    other = 1 - me
    place = lax.axis_index("sp")
    half = tok.shape[1]
    total_rows = normed.shape[0]
    width = w_key.shape[1]
    heads = init_memory.shape[0]
    dh = init_memory.shape[1]
    nblocks = total_rows // BLOCK
    key_factor = dh ** (-0.5)
    out_width = layer_out.shape[1]
    n_out = half // BLOCK
    out_cols = out_width // n_out

    barrier = pltpu.get_barrier_semaphore()
    pl.semaphore_signal(barrier, inc=1, device_id={"tp": other}, device_id_type=MESH)
    for d in range(1, n_sp):
        pl.semaphore_signal(
            barrier, inc=1, device_id={"sp": lax.rem(place + d, n_sp)}, device_id_type=MESH
        )

    own_copy = pltpu.make_async_copy(tokens, tok.at[0], local_sem.at[0])
    own_copy.start()
    w_in = (w_key, w_value, w_gatein, w_convin, w_gateout, w_query, w_outgate)
    w_copies = [
        pltpu.make_async_copy(w, weights.at[s], weight_sem.at[s]) for s, w in enumerate(w_in)
    ]
    out_copies = [
        pltpu.make_async_copy(out_memory, out_w.at[pl.ds(0, width)], weight_sem.at[7]),
        pltpu.make_async_copy(out_conv, out_w.at[pl.ds(width, width)], weight_sem.at[8]),
    ]
    for c in w_copies + out_copies:
        c.start()

    pl.semaphore_wait(barrier, n_sp)
    token_copy = pltpu.make_async_remote_copy(
        src_ref=tokens,
        dst_ref=tok.at[1],
        send_sem=token_sem.at[0],
        recv_sem=token_sem.at[1],
        device_id={"tp": other},
        device_id_type=MESH,
    )
    token_copy.start()

    gates = jnp.concatenate(
        [w_fgate[...], w_igate[...], jnp.zeros((BLOCK - 2 * PAD, w_igate.shape[1]), BF16)], axis=0
    )
    gate_w[...] = jnp.transpose(gates)
    for j in range(norm_gain.shape[0]):
        gain_row[:, j * BLOCK : (j + 1) * BLOCK] = norm_gain[j : j + 1].astype(F32)
    head_rows[...] = head_gain[...].astype(F32)
    own_copy.wait()

    def rows_of(index, size):
        return pl.ds(pl.multiple_of(index * size, size), size)

    def normalize(slot, base):
        @pl.loop(0, half // NORM_ROWS)
        def _(c):
            x = tok[slot, rows_of(c, NORM_ROWS), :].astype(F32)
            scale = lax.rsqrt(jnp.mean(x * x, axis=-1, keepdims=True) + EPSILON)
            y = (x * scale) * gain_row[...]
            normed[pl.ds(pl.multiple_of(base + c * NORM_ROWS, NORM_ROWS), NORM_ROWS), :] = y.astype(
                BF16
            )

    def project(slot, rows):
        proj[slot, rows, :] = jnp.dot(
            normed[rows, :], weights[slot], preferred_element_type=F32
        ).astype(BF16)

    @pl.loop(0, 2)
    def _(step):
        index = lax.rem(me + step, 2)

        @pl.when(step == 1)
        def _():
            token_copy.wait_recv()

        normalize(step, index * half)
        rows = rows_of(index, half)
        gate_pre[rows, :] = jnp.dot(normed[rows, :], gate_w[...], preferred_element_type=F32)

        @pl.loop(KEY, VALUE + 1)
        def _(slot):
            @pl.when(step == 0)
            def _():
                pltpu.make_async_copy(w_key, weights.at[slot], weight_sem.at[slot]).wait()

            project(slot, rows)

    row_i = lax.broadcasted_iota(jnp.int32, (BLOCK, BLOCK), 0)
    col_i = lax.broadcasted_iota(jnp.int32, (BLOCK, BLOCK), 1)
    upper = jnp.where(row_i <= col_i, 1.0, 0.0).astype(F32)
    for h in range(heads):
        running[h] = jnp.zeros((dh, dh), F32)
    running_log[0:PAD] = jnp.full((PAD, BLOCK), LOWEST_LOG, F32)
    running_log[PAD : 2 * PAD] = jnp.zeros((PAD, BLOCK), F32)

    def head_cols(h):
        return slice(h * dh, (h + 1) * dh)

    first_head = me * heads
    to_front = lax.rem(PAD - first_head, PAD)
    lane_head = lax.broadcasted_iota(jnp.int32, (PAD, BLOCK), 0)
    bias_f = jnp.zeros((PAD, BLOCK), F32)
    bias_i = jnp.zeros((PAD, BLOCK), F32)
    for h in range(heads):
        bias_f = jnp.where(lane_head == h, forget_bias[first_head + h], bias_f)
        bias_i = jnp.where(lane_head == h, input_bias[first_head + h], bias_i)
    no_head = jnp.zeros((PAD - heads, BLOCK), F32)

    forget_rows, in_rows = [], []
    for b in range(nblocks):
        span = slice(b * BLOCK, (b + 1) * BLOCK)
        pre = jnp.transpose(gate_pre[span, :])
        v = pltpu.roll(pre[0:PAD], to_front, 0) + bias_f
        log_forget = jnp.minimum(v, 0.0) - jnp.log1p(jnp.exp(-jnp.abs(v)))
        forget_rows.append(log_forget + jnp.concatenate([extra[:, span], no_head], axis=0))
        in_rows.append(pltpu.roll(pre[PAD : 2 * PAD], to_front, 0) + bias_i)
    all_cumulative = jnp.dot(
        jnp.concatenate(forget_rows, axis=0),
        upper,
        precision=lax.Precision.HIGHEST,
        preferred_element_type=F32,
    )
    all_in = jnp.concatenate(in_rows, axis=0)
    all_total = jnp.broadcast_to(all_cumulative[:, BLOCK - 1 : BLOCK], all_in.shape)
    exponent = all_total - all_cumulative + all_in
    all_peak = jnp.broadcast_to(jnp.max(exponent, axis=1, keepdims=True), all_in.shape)
    key_weight = jnp.exp(exponent - all_peak)
    filler = jnp.zeros((BLOCK - 2 * PAD, BLOCK), F32)
    for b in range(nblocks):
        span = slice(b * PAD, (b + 1) * PAD)
        row_log[b, 0:PAD] = all_cumulative[span]
        row_log[b, PAD : 2 * PAD] = all_in[span]
        block_sum[b] = all_total[span]
        block_peak[b] = all_peak[span]
        col_log[b] = jnp.transpose(
            jnp.concatenate([all_cumulative[span], key_weight[span], filler], axis=0)
        )

    @pl.loop(0, nblocks, unroll=2)
    def _(b):
        rows = rows_of(b, BLOCK)
        columns = col_log[b]
        total, peak = block_sum[b], block_peak[b]
        old_log = running_log[0:PAD]
        merged = jnp.maximum(total + old_log, peak)
        keep = jnp.exp(total + old_log - merged)
        add = jnp.exp(peak - merged)
        running_log[0:PAD] = merged
        running_log[PAD : 2 * PAD] = running_log[PAD : 2 * PAD] + total
        for h in range(heads):
            k = proj[KEY, rows, head_cols(h)].astype(F32)
            wk = (columns[:, PAD + h : PAD + h + 1] * k * key_factor).astype(BF16)
            term = lax.dot_general(
                wk,
                proj[VALUE, rows, head_cols(h)],
                (((0,), (0,)), ((), ())),
                preferred_element_type=F32,
            )
            terms[b, h] = term
            running[h] = keep[h : h + 1] * running[h] + add[h : h + 1] * term

    for h in range(heads):
        seg_memory[h] = running[h].astype(BF16)
    seg_log[...] = running_log[...]

    def seg_copies(target, source, d):
        return [
            pltpu.make_async_remote_copy(
                src_ref=src,
                dst_ref=dst.at[source],
                send_sem=seg_send.at[which, d],
                recv_sem=seg_recv.at[which, source],
                device_id={"sp": target},
                device_id_type=MESH,
            )
            for which, (src, dst) in enumerate(((seg_memory, got_memory), (seg_log, got_log)))
        ]

    for d in range(1, n_sp):

        @pl.when(place + d < n_sp)
        def _(d=d):
            for c in seg_copies(place + d, place, d - 1):
                c.start()

    def finish(slots):
        @pl.loop(slots[0], slots[1])
        def _(slot):
            pltpu.make_async_copy(w_key, weights.at[slot], weight_sem.at[slot]).wait()

            @pl.loop(0, 2)
            def _(index):
                project(slot, rows_of(index, half))

    finish((GATE_IN, CONV_IN + 1))

    @pl.loop(0, nblocks)
    def _(b):
        rows = rows_of(b, BLOCK)
        product = proj[GATE_IN, rows, :].astype(F32) * proj[CONV_IN, rows, :].astype(F32)
        conv_rows[pl.ds(pl.multiple_of(RIM + b * BLOCK, RIM), BLOCK), :] = product.astype(BF16)

    next_place = lax.rem(place + 1, n_sp)
    rim_copy = pltpu.make_async_remote_copy(
        src_ref=conv_rows.at[pl.ds(total_rows, RIM)],
        dst_ref=rim,
        send_sem=rim_sem.at[0],
        recv_sem=rim_sem.at[1],
        device_id={"sp": next_place},
        device_id_type=MESH,
    )

    @pl.when(place + 1 < n_sp)
    def _():
        rim_copy.start()

    finish((GATE_OUT, OUT_GATE + 1))

    @pl.when(place > 0)
    def _():
        rim_copy.wait_recv()
        conv_rows[0:RIM, :] = rim[...]

    @pl.when(place == 0)
    def _():
        conv_rows[0:RIM, :] = jnp.zeros((RIM, width), BF16)

    own_cols = pl.ds(pl.multiple_of(me * width, width), width)
    taps = conv_taps[:, own_cols].astype(F32)
    tap_count = conv_taps.shape[0]

    @pl.loop(0, nblocks)
    def _(b):
        rows = rows_of(b, BLOCK)
        x = conv_rows[pl.ds(pl.multiple_of(b * BLOCK, RIM), BLOCK + RIM), :].astype(F32)
        mixed = None
        for j in range(tap_count):
            back = tap_count - 1 - j
            y = x if back == 0 else pltpu.roll(x, back, 0)
            y = y[RIM:] * taps[j : j + 1]
            mixed = y if mixed is None else mixed + y
        mix[rows, pl.ds(width, width)] = (proj[GATE_OUT, rows, :].astype(F32) * mixed).astype(BF16)

    for h in range(heads):
        running[h] = init_memory[h]
    running_log[0:PAD] = jnp.zeros((PAD, BLOCK), F32)

    def advance(total, peak, term_of):
        old_log = running_log[0:PAD]
        merged = jnp.maximum(total + old_log, peak)
        keep = jnp.exp(total + old_log - merged)
        add = jnp.exp(peak - merged)
        running_log[0:PAD] = merged
        for h in range(heads):
            running[h] = keep[h : h + 1] * running[h] + add[h : h + 1] * term_of(h)

    @pl.loop(0, place)
    def _(source):
        for c in seg_copies(place, source, 0):
            c.wait_recv()
        advance(
            got_log[source, PAD : 2 * PAD],
            got_log[source, 0:PAD],
            lambda h: got_memory[source, h].astype(F32),
        )

    @pl.loop(0, nblocks)
    def _(b):
        starts_log[b] = running_log[0:PAD]
        for h in range(heads):
            starts[b, h] = running[h].astype(BF16)
        advance(block_sum[b], block_peak[b], lambda h: terms[b, h])

    causal = col_i <= row_i

    def read_block(b):
        rows = rows_of(b, BLOCK)
        columns = col_log[b]
        for h in range(heads):
            q = proj[QUERY, rows, head_cols(h)]
            k = proj[KEY, rows, head_cols(h)]
            scores = lax.dot_general(
                q, k, (((1,), (1,)), ((), ())), preferred_element_type=F32
            )
            cum_col = columns[:, h : h + 1]
            pair = (cum_col - row_log[b, h : h + 1]) + row_log[b, PAD + h : PAD + h + 1]
            pair = jnp.where(causal, pair, -jnp.inf)
            carried_log = cum_col + starts_log[b, h : h + 1, 0:1]
            top = jnp.maximum(carried_log, jnp.max(pair, axis=1, keepdims=True))
            weighted = (jnp.exp(pair - top) * (scores * key_factor)).astype(BF16)
            carried = jnp.dot(q, starts[b, h], preferred_element_type=F32)
            out = jnp.exp(carried_log - top) * carried + jnp.dot(
                weighted, proj[VALUE, rows, head_cols(h)], preferred_element_type=F32
            )
            out = out * lax.rsqrt(jnp.mean(out * out, axis=1, keepdims=True) + EPSILON)
            gate = jax.nn.sigmoid(proj[OUT_GATE, rows, head_cols(h)].astype(F32))
            mix[rows, head_cols(h)] = (out * head_rows[pl.ds(first_head + h, 1), :] * gate).astype(BF16)

    def part_copy(c):
        return pltpu.make_async_remote_copy(
            src_ref=part_send.at[c],
            dst_ref=part_got.at[c],
            send_sem=part_sem_send.at[c],
            recv_sem=part_sem_recv.at[c],
            device_id={"tp": other},
            device_id_type=MESH,
        )

    def partial_rows(index, c):
        return jnp.dot(
            mix[rows_of(index, half), :], out_w[:, rows_of(c, out_cols)], preferred_element_type=F32
        ).astype(BF16)

    @pl.loop(0, n_out)
    def _(step):
        read_block(other * n_out + step)

    for c in out_copies:
        c.wait()

    @pl.loop(0, n_out)
    def _(step):
        part_send[step] = partial_rows(other, step)
        read_block(me * n_out + step)
        part_copy(step).start()

    @pl.loop(0, n_out)
    def _(c):
        own = partial_rows(me, c)
        part_copy(c).wait_recv()
        total = own.astype(F32) + part_got[c].astype(F32)
        layer_out[:, rows_of(c, out_cols)] = total.astype(BF16)

    token_copy.wait_send()

    @pl.when(place + 1 < n_sp)
    def _():
        rim_copy.wait_send()

    for d in range(1, n_sp):

        @pl.when(place + d < n_sp)
        def _(d=d):
            for c in seg_copies(place + d, place, d - 1):
                c.wait_send()

    @pl.loop(0, n_out)
    def _(c):
        part_copy(c).wait_send()


def local(
    tokens,
    norm_gain,
    w_query,
    w_key,
    w_value,
    w_outgate,
    w_gatein,
    w_gateout,
    w_convin,
    w_igate,
    w_fgate,
    input_bias,
    forget_bias,
    forget_extra,
    init_memory,
    head_gain,
    conv_taps,
    out_memory,
    out_conv,
):
    heads, dh = init_memory.shape[1], init_memory.shape[2]
    half, features = tokens.shape[1], tokens.shape[2]
    rows = forget_extra.shape[1]
    width = w_query.shape[1]
    nblocks = rows // BLOCK
    n_sp = lax.axis_size("sp")
    vmem = pl.BlockSpec(memory_space=pltpu.VMEM)
    hbm = pl.BlockSpec(memory_space=pl.ANY)
    smem = pl.BlockSpec(memory_space=pltpu.SMEM)
    dma = pltpu.SemaphoreType.DMA
    n_seg = max(n_sp - 1, 1)
    n_out = half // BLOCK
    out_cols = features // n_out
    out = pl.pallas_call(
        functools.partial(kernel, n_sp),
        name="layer",
        out_shape=pltpu.VMEM((half, features), BF16),
        in_specs=[hbm, vmem] + [hbm] * 7 + [vmem] * 2 + [smem] * 2 + [vmem] * 4 + [hbm] * 2,
        out_specs=vmem,
        scratch_shapes=[
            pltpu.VMEM((2, half, features), BF16),
            pltpu.VMEM((1, features), F32),
            pltpu.VMEM((PAD, BLOCK), F32),
            pltpu.VMEM((features, BLOCK), BF16),
            pltpu.VMEM((rows, features), BF16),
            pltpu.VMEM((7, features, width), BF16),
            pltpu.VMEM((2 * width, features), BF16),
            pltpu.VMEM((7, rows, width), BF16),
            pltpu.VMEM((rows, BLOCK), F32),
            pltpu.VMEM((nblocks, 2 * PAD, BLOCK), F32),
            pltpu.VMEM((nblocks, BLOCK, BLOCK), F32),
            pltpu.VMEM((nblocks, PAD, BLOCK), F32),
            pltpu.VMEM((nblocks, PAD, BLOCK), F32),
            pltpu.VMEM((nblocks, heads, dh, dh), F32),
            pltpu.VMEM((heads, dh, dh), F32),
            pltpu.VMEM((2 * PAD, BLOCK), F32),
            pltpu.VMEM((nblocks, heads, dh, dh), BF16),
            pltpu.VMEM((nblocks, PAD, BLOCK), F32),
            pltpu.VMEM((heads, dh, dh), BF16),
            pltpu.VMEM((2 * PAD, BLOCK), F32),
            pltpu.VMEM((n_seg, heads, dh, dh), BF16),
            pltpu.VMEM((n_seg, 2 * PAD, BLOCK), F32),
            pltpu.VMEM((RIM + rows, width), BF16),
            pltpu.VMEM((RIM, width), BF16),
            pltpu.VMEM((rows, 2 * width), BF16),
            pltpu.VMEM((n_out, half, out_cols), BF16),
            pltpu.VMEM((n_out, half, out_cols), BF16),
            dma((1,)),
            dma((9,)),
            dma((2,)),
            dma((2, n_seg)),
            dma((2, n_seg)),
            dma((2,)),
            dma((n_out,)),
            dma((n_out,)),
        ],
        compiler_params=pltpu.CompilerParams(
            collective_id=0, has_side_effects=True, vmem_limit_bytes=60 * 1024 * 1024
        ),
    )(
        tokens[0],
        norm_gain.reshape(-1, BLOCK),
        w_key,
        w_value,
        w_gatein,
        w_convin,
        w_gateout,
        w_query,
        w_outgate,
        jnp.transpose(w_igate),
        jnp.transpose(w_fgate),
        input_bias,
        forget_bias,
        jnp.transpose(forget_extra[0]),
        init_memory[0],
        head_gain.reshape(-1, dh),
        conv_taps,
        out_memory,
        out_conv,
    )
    return out[None]


def solution(mesh):
    return jax.shard_map(
        local,
        mesh=mesh,
        in_specs=(
            P("fs", ("sp", "tp"), None),
            P(),
            P(None, "tp"),
            P(None, "tp"),
            P(None, "tp"),
            P(None, "tp"),
            P(None, "tp"),
            P(None, "tp"),
            P(None, "tp"),
            P(),
            P(),
            P(),
            P(),
            P("fs", "sp", "tp"),
            P("fs", "tp", None, None),
            P(),
            P(),
            P("tp", None),
            P("tp", None),
        ),
        out_specs=P("fs", ("sp", "tp"), None),
        check_vma=False,
    )
```

profile of v0, /device:TPU:10, one launch (start us, length us, event | category | flops | bytes accessed | tf_op | source)
XLA Modules:
  0.0 47.5 jit_solution(14435158206336123296)
XLA Ops:
  0.0 46.2 %layer.1 = bf16[512,2048]{1,0:T(8,128)(2,1)S(1)} custom-call(bf16[512,2048]{1,0:T(8,128)(2,1)} %bitcast.11, bf16[16,128]{1,0:T(8,128)(2,1)} %bitcast.16, bf16[2048,512]{1,0:T(8,128)(2,1)} %w_key.1, bf16[2048,512]{1,0:T(8,128)(2,1)} %w_value.1, bf16[2048,512]{1,0:T(8,128)(2,1)} %w_gatein.1, bf16[2048,512]{1,0:T(8,128)(2,1)} %w_convin.1, ...), custom_call_target="tpu_custom_call" | custom-call | tf_op jit(solution)/shard_map/layer/pallas_call | solution.py:471
  46.2 1.3 %copy.21 = bf16[1,512,2048]{2,1,0:T(8,128)(2,1)} copy(bf16[1,512,2048]{2,1,0:T(8,128)(2,1)S(1)} %bitcast.10) | data formatting | bytes 4194304
where the time goes:
time: 48.4 us; the launch traced here: 47.5 us
  Pallas kernels  46.2 us (95%)
  local copies, waits for them, and re-layouts  1.32 us (3%)
    pallas_call x1, Pallas kernels, local(): pl.pallas_call(functools.partial(kernel, n_sp), name='layer', out_shape=p...  46.2 us
    unnamed x1, local copies, waits for them, and re-layouts  1.32 us

commit v1 on v0

v1 whole, which is shorter than its diff:
```python
import functools

import jax
import jax.numpy as jnp
from jax import lax
from jax.experimental import pallas as pl
from jax.experimental.pallas import tpu as pltpu
from jax.sharding import PartitionSpec as P

BLOCK = 128
EPSILON = 1e-06
LOWEST_LOG = -1e30
MESH = pl.DeviceIdType.MESH
F32 = jnp.float32
BF16 = jnp.bfloat16
PAD = 8
RIM = 16
NORM_ROWS = 64
BATCHES = 2

KEY, VALUE, QUERY, GATE_IN, CONV_IN, GATE_OUT, OUT_GATE = range(7)


def kernel(
    n_sp,
    tokens,
    norm_gain,
    w_key,
    w_value,
    w_query,
    w_gatein,
    w_convin,
    w_gateout,
    w_outgate,
    w_igate,
    w_fgate,
    input_bias,
    forget_bias,
    extra_in,
    init_in,
    head_gain,
    taps_in,
    out_memory,
    out_conv,
    layer_out,
    tok,
    gain_in,
    gain_row,
    head_in,
    head_rows,
    igate_in,
    fgate_in,
    gate_w,
    bias_in,
    extra,
    init_memory,
    conv_taps,
    normed,
    weights,
    out_m,
    out_c,
    k_rows,
    v_rows,
    q_rows,
    conv_pair,
    go_rows,
    og_rows,
    gate_pre,
    row_log,
    col_log,
    block_sum,
    block_peak,
    prefix,
    prefix_cols,
    half_sum,
    half_log,
    half_total,
    relay_rows,
    carry,
    carry_log,
    carry_cols,
    send_memory,
    send_log,
    local_out,
    local_top,
    conv_rows,
    rim,
    rim_out,
    mix_conv,
    mix_memory,
    acc,
    token_sem,
    small_sem,
    weight_sem,
    norm_send,
    norm_recv,
    outw_send,
    outw_recv,
    state_send,
    state_recv,
    rim_sem,
    conv_sem,
    mem_send,
    mem_recv,
):
    me = lax.axis_index("tp")
    other = 1 - me
    place = lax.axis_index("sp")
    half = tok.shape[0]
    total_rows = normed.shape[0]
    width = k_rows.shape[1]
    heads = init_memory.shape[0]
    dh = init_memory.shape[1]
    n_half = half // BLOCK
    nblocks = total_rows // BLOCK
    key_factor = dh ** (-0.5)
    out_width = layer_out.shape[1]
    n_out = n_half
    out_cols = out_width // n_out
    group = heads // BATCHES

    barrier = pltpu.get_barrier_semaphore()
    pl.semaphore_signal(barrier, inc=1, device_id={"tp": other}, device_id_type=MESH)

    @pl.when(place > 0)
    def _():
        pl.semaphore_signal(barrier, inc=1, device_id={"sp": place - 1}, device_id_type=MESH)

    def rows_of(index, size):
        return pl.ds(pl.multiple_of(index * size, size), size)

    tok_copies = [
        pltpu.make_async_copy(
            tokens.at[pl.ds(c * BLOCK, BLOCK)], tok.at[pl.ds(c * BLOCK, BLOCK)], token_sem.at[c]
        )
        for c in range(n_half)
    ]
    smalls = [
        pltpu.make_async_copy(src, dst, small_sem.at[i])
        for i, (src, dst) in enumerate(
            (
                (norm_gain, gain_in),
                (w_igate, igate_in),
                (w_fgate, fgate_in),
                (input_bias, bias_in.at[0]),
                (forget_bias, bias_in.at[1]),
                (extra_in, extra),
                (init_in, init_memory),
                (head_gain, head_in),
                (taps_in, conv_taps),
            )
        )
    ]
    w_in = (w_key, w_value, w_query, w_gatein, w_convin, w_gateout, w_outgate)
    w_copies = [
        pltpu.make_async_copy(w, weights.at[s], weight_sem.at[s]) for s, w in enumerate(w_in)
    ]
    out_copies = [
        pltpu.make_async_copy(out_memory, out_m.at[pl.ds(0, width)], weight_sem.at[7]),
        pltpu.make_async_copy(out_conv, out_c.at[pl.ds(0, width)], weight_sem.at[8]),
    ]

    def partner_copy(src, dst, send_sem, recv_sem):
        return pltpu.make_async_remote_copy(
            src_ref=src,
            dst_ref=dst,
            send_sem=send_sem,
            recv_sem=recv_sem,
            device_id={"tp": other},
            device_id_type=MESH,
        )

    def norm_copy(c):
        rows = pl.ds(pl.multiple_of(me * half + c * BLOCK, BLOCK), BLOCK)
        return partner_copy(normed.at[rows], normed.at[rows], norm_send.at[c], norm_recv.at[c])

    outw_copies = [
        partner_copy(src, dst.at[pl.ds(width, width)], outw_send.at[i], outw_recv.at[i])
        for i, (src, dst) in enumerate(((out_conv, out_c), (out_memory, out_m)))
    ]

    smalls[0].start()
    for c in tok_copies:
        c.start()
    for c in smalls[1:]:
        c.start()

    smalls[0].wait()
    for j in range(norm_gain.shape[0]):
        gain_row[:, j * BLOCK : (j + 1) * BLOCK] = gain_in[j : j + 1].astype(F32)

    def normalize(c):
        @pl.loop(0, BLOCK // NORM_ROWS)
        def _(part):
            start = c * BLOCK + part * NORM_ROWS
            x = tok[pl.ds(pl.multiple_of(start, NORM_ROWS), NORM_ROWS), :].astype(F32)
            scale = lax.rsqrt(jnp.mean(x * x, axis=-1, keepdims=True) + EPSILON)
            y = (x * scale) * gain_row[...]
            normed[pl.ds(pl.multiple_of(me * half + start, NORM_ROWS), NORM_ROWS), :] = y.astype(
                BF16
            )

    first_weights = 3
    smalls[1].wait()
    smalls[2].wait()
    gates = jnp.concatenate(
        [
            fgate_in[...],
            igate_in[...],
            jnp.zeros((BLOCK - 2 * PAD, igate_in.shape[1]), BF16),
        ],
        axis=0,
    )
    gate_w[...] = jnp.transpose(gates)
    for c in range(n_half):
        tok_copies[c].wait()
        if c < first_weights:
            w_copies[c].start()
        normalize(c)
    for c in w_copies[min(first_weights, n_half) :]:
        c.start()

    for c in smalls[3:]:
        c.wait()
    head_rows[...] = head_in[...].astype(F32)

    @pl.when(place == 0)
    def _():
        for h in range(heads):
            carry[0, h] = init_memory[h].astype(BF16)
        carry_log[0] = jnp.zeros((PAD, BLOCK), F32)

    row_i = lax.broadcasted_iota(jnp.int32, (BLOCK, BLOCK), 0)
    col_i = lax.broadcasted_iota(jnp.int32, (BLOCK, BLOCK), 1)
    upper = jnp.where(row_i <= col_i, 1.0, 0.0).astype(F32)
    causal = col_i <= row_i

    def head_cols(h):
        return slice(h * dh, (h + 1) * dh)

    first_head = me * heads
    to_front = lax.rem(PAD - first_head, PAD)
    lane_head = lax.broadcasted_iota(jnp.int32, (PAD, BLOCK), 0)
    bias_f = jnp.zeros((PAD, BLOCK), F32)
    bias_i = jnp.zeros((PAD, BLOCK), F32)
    for h in range(heads):
        bias_i = jnp.where(lane_head == h, bias_in[0, first_head + h], bias_i)
        bias_f = jnp.where(lane_head == h, bias_in[1, first_head + h], bias_f)
    no_head = jnp.zeros((PAD - heads, BLOCK), F32)

    def dot(a, b):
        return jnp.dot(a, b, preferred_element_type=F32)

    def project(target, slot, rows):
        target[rows, :] = dot(normed[rows, :], weights[slot]).astype(BF16)

    def gate_math(index):
        forget_rows, in_rows = [], []
        for j in range(n_half):
            span = rows_of(index * n_half + j, BLOCK)
            pre = jnp.transpose(gate_pre[span, :])
            v = pltpu.roll(pre[0:PAD], to_front, 0) + bias_f
            log_forget = jnp.minimum(v, 0.0) - jnp.log1p(jnp.exp(-jnp.abs(v)))
            forget_rows.append(log_forget + jnp.concatenate([extra[:, span], no_head], axis=0))
            in_rows.append(pltpu.roll(pre[PAD : 2 * PAD], to_front, 0) + bias_i)
        all_cumulative = jnp.dot(
            jnp.concatenate(forget_rows, axis=0),
            upper,
            precision=lax.Precision.HIGHEST,
            preferred_element_type=F32,
        )
        all_in = jnp.concatenate(in_rows, axis=0)
        all_total = jnp.broadcast_to(all_cumulative[:, BLOCK - 1 : BLOCK], all_in.shape)
        exponent = all_total - all_cumulative + all_in
        all_peak = jnp.broadcast_to(jnp.max(exponent, axis=1, keepdims=True), all_in.shape)
        key_weight = jnp.exp(exponent - all_peak) * key_factor
        filler = jnp.zeros((BLOCK - 2 * PAD, BLOCK), F32)
        for j in range(n_half):
            b = index * n_half + j
            span = slice(j * PAD, (j + 1) * PAD)
            row_log[b, 0:PAD] = all_cumulative[span]
            row_log[b, PAD : 2 * PAD] = all_in[span]
            block_sum[b] = all_total[span]
            block_peak[b] = all_peak[span]
            col_log[b] = jnp.transpose(
                jnp.concatenate([all_cumulative[span], key_weight[span], filler], axis=0)
            )

    def half_state(index):
        log = jnp.full((PAD, BLOCK), LOWEST_LOG, F32)
        total = jnp.zeros((PAD, BLOCK), F32)
        filler = jnp.zeros((BLOCK - 2 * PAD, BLOCK), F32)
        keeps, adds = [], []
        for j in range(n_half):
            b = index * n_half + j
            prefix_cols[b] = jnp.transpose(jnp.concatenate([log, total, filler], axis=0))
            now, peak = block_sum[b], block_peak[b]
            merged = jnp.maximum(now + log, peak)
            keeps.append(jnp.exp(now + log - merged))
            adds.append(jnp.exp(peak - merged))
            log = merged
            total = total + now
        half_log[index] = log
        half_total[index] = total
        for h in range(heads):
            state = jnp.zeros((dh, dh), F32)
            for j in range(n_half):
                b = index * n_half + j
                rows = rows_of(b, BLOCK)
                prefix[b, h] = state.astype(BF16)
                k = k_rows[rows, head_cols(h)].astype(F32)
                wk = (col_log[b, :, PAD + h : PAD + h + 1] * k).astype(BF16)
                term = lax.dot_general(
                    wk,
                    v_rows[rows, head_cols(h)],
                    (((0,), (0,)), ((), ())),
                    preferred_element_type=F32,
                )
                state = keeps[j][h : h + 1] * state + adds[j][h : h + 1] * term
            half_sum[index, h] = state

    own_rows = rows_of(me, half)
    gate_pre[own_rows, :] = dot(normed[own_rows, :], gate_w[...])
    pl.semaphore_wait(barrier, jnp.where(place + 1 < n_sp, 2, 1))
    for c in range(n_half):
        norm_copy(c).start()

    @pl.loop(0, 2)
    def _(step):
        index = lax.rem(me + step, 2)
        rows = rows_of(index, half)

        @pl.when(step == 0)
        def _():
            w_copies[KEY].wait()

        @pl.when(step == 1)
        def _():
            for c in range(n_half):
                norm_copy(c).wait_recv()
            gate_pre[rows, :] = dot(normed[rows, :], gate_w[...])

        project(k_rows, KEY, rows)

        @pl.when(step == 0)
        def _():
            w_copies[VALUE].wait()
            for c in out_copies:
                c.start()
            for c in outw_copies:
                c.start()

        project(v_rows, VALUE, rows)
        gate_math(index)

        @pl.when(step == 0)
        def _():
            w_copies[QUERY].wait()

        project(q_rows, QUERY, rows)
        half_state(index)

    for c in w_copies[GATE_IN:]:
        c.wait()

    def state_copies(k):
        span = pl.ds(k * group, group)
        pairs = [(send_memory.at[span], carry.at[0, span], k)]
        if k == 0:
            pairs.append((send_log, carry_log.at[0], BATCHES))
        return [
            pltpu.make_async_remote_copy(
                src_ref=src,
                dst_ref=dst,
                send_sem=state_send.at[s],
                recv_sem=state_recv.at[s],
                device_id={"sp": lax.rem(place + 1, n_sp)},
                device_id_type=MESH,
            )
            for src, dst, s in pairs
        ]

    def relay(k):
        @pl.when(place > 0)
        def _():
            for c in state_copies(k):
                c.wait_recv()

        if k == 0:
            log = carry_log[0]
            for i in range(2):
                now, peak = half_total[i], half_log[i]
                merged = jnp.maximum(now + log, peak)
                relay_rows[2 * i] = jnp.exp(now + log - merged)
                relay_rows[2 * i + 1] = jnp.exp(peak - merged)
                filler = jnp.zeros((BLOCK - PAD, BLOCK), F32)
                carry_cols[i] = jnp.transpose(jnp.concatenate([log, filler], axis=0))
                log = merged
            send_log[...] = log
        for h in range(k * group, (k + 1) * group):
            state = carry[0, h].astype(F32)
            for i in range(2):
                keep = relay_rows[2 * i, h : h + 1]
                add = relay_rows[2 * i + 1, h : h + 1]
                state = keep * state + add * half_sum[i, h]
                if i == 0:
                    carry[1, h] = state.astype(BF16)
            send_memory[h] = state.astype(BF16)

        @pl.when(place + 1 < n_sp)
        def _():
            for c in state_copies(k):
                c.start()

    n_main = 2 * n_half

    def relays(g):
        for k in range(BATCHES):
            due = jnp.where(place == 0, 0, jnp.minimum(2 * place + k, n_main))

            @pl.when(due == g)
            def _(k=k):
                relay(k)

    def read_block(b):
        rows = rows_of(b, BLOCK)
        columns = col_log[b]
        carried_all = columns + prefix_cols[b]
        tops = jnp.zeros((BLOCK, BLOCK), F32)
        for h in range(heads):
            q = q_rows[rows, head_cols(h)]
            k = k_rows[rows, head_cols(h)]
            scores = lax.dot_general(
                q, k, (((1,), (1,)), ((), ())), preferred_element_type=F32
            )
            carried = dot(q, prefix[b, h])
            pair = (columns[:, h : h + 1] - row_log[b, h : h + 1]) + row_log[
                b, PAD + h : PAD + h + 1
            ]
            pair = jnp.where(causal, pair, -jnp.inf)
            carried_log = carried_all[:, h : h + 1]
            top = jnp.maximum(carried_log, jnp.max(pair, axis=1, keepdims=True))
            weighted = (jnp.exp(pair - top) * (scores * key_factor)).astype(BF16)
            local_out[rows, head_cols(h)] = jnp.exp(carried_log - top) * carried + dot(
                weighted, v_rows[rows, head_cols(h)]
            )
            tops = jnp.where(col_i == h, top, tops)
        local_top[b] = tops

    taps_cols = pl.ds(pl.multiple_of(me * width, width), width)
    taps = conv_taps[:, taps_cols].astype(F32)
    tap_count = conv_taps.shape[0]

    def product(rows):
        return (conv_pair[0, rows, :].astype(F32) * conv_pair[1, rows, :].astype(F32)).astype(BF16)

    split = n_main // 2

    @pl.loop(0, split)
    def _(g):
        relays(g)
        slot = lax.div(g, n_half // 2)
        project(conv_pair.at[slot], GATE_IN + slot, rows_of(lax.rem(g, 2), half))
        read_block(g)

    rim_out[...] = product(pl.ds(total_rows - RIM, RIM))
    rim_copy = pltpu.make_async_remote_copy(
        src_ref=rim_out,
        dst_ref=rim,
        send_sem=rim_sem.at[0],
        recv_sem=rim_sem.at[1],
        device_id={"sp": lax.rem(place + 1, n_sp)},
        device_id_type=MESH,
    )

    @pl.when(place + 1 < n_sp)
    def _():
        rim_copy.start()

    @pl.loop(split, split + 2)
    def _(g):
        relays(g)
        index = g - split
        for j in range(n_half):
            b = index * n_half + j
            target = pl.ds(pl.multiple_of(RIM + b * BLOCK, RIM), BLOCK)
            conv_rows[target, :] = product(rows_of(b, BLOCK))
        project(go_rows, GATE_OUT, rows_of(index, half))
        read_block(g)

    @pl.when(place > 0)
    def _():
        rim_copy.wait_recv()
        conv_rows[0:RIM, :] = rim[...]

    @pl.when(place == 0)
    def _():
        conv_rows[0:RIM, :] = jnp.zeros((RIM, width), BF16)

    conv_copy = partner_copy(
        mix_conv.at[1, :, pl.ds(0, width)],
        mix_conv.at[0, :, pl.ds(width, width)],
        conv_sem.at[0],
        conv_sem.at[1],
    )

    @pl.loop(split + 2, n_main)
    def _(g):
        relays(g)
        turn = g - (split + 2)
        side = jnp.where(turn == 0, other, me)
        for j in range(n_half):
            b = side * n_half + j
            x = conv_rows[pl.ds(pl.multiple_of(b * BLOCK, RIM), BLOCK + RIM), :].astype(F32)
            mixed = None
            for t in range(tap_count):
                back = tap_count - 1 - t
                y = x if back == 0 else pltpu.roll(x, back, 0)
                y = y[RIM:] * taps[t : t + 1]
                mixed = y if mixed is None else mixed + y
            mix_conv[1 - turn, pl.ds(j * BLOCK, BLOCK), pl.ds(0, width)] = (
                go_rows[rows_of(b, BLOCK), :].astype(F32) * mixed
            ).astype(BF16)
        project(og_rows, OUT_GATE, rows_of(turn, half))
        read_block(g)

        @pl.when(turn == 0)
        def _():
            conv_copy.start()

    relays(n_main)
    for c in out_copies:
        c.wait()
    for c in outw_copies:
        c.wait_recv()
    conv_copy.wait_recv()

    def finish_block(side, slot, j):
        b = side * n_half + j
        rows = rows_of(b, BLOCK)
        local = local_top[b]
        carried_all = (
            col_log[b] + pltpu.roll(prefix_cols[b], BLOCK - PAD, 1) + carry_cols[side]
        )
        top = jnp.maximum(local, carried_all)
        local_factor = jnp.exp(local - top)
        carried_factor = jnp.exp(carried_all - top)
        for h in range(heads):
            q = q_rows[rows, head_cols(h)]
            out = carried_factor[:, h : h + 1] * dot(q, carry[side, h]) + local_factor[
                :, h : h + 1
            ] * local_out[rows, head_cols(h)]
            out = out * lax.rsqrt(jnp.mean(out * out, axis=1, keepdims=True) + EPSILON)
            gate = jax.nn.sigmoid(og_rows[rows, head_cols(h)].astype(F32))
            mix_memory[slot, rows_of(j, BLOCK), head_cols(h)] = (
                out * head_rows[pl.ds(first_head + h, 1), :] * gate
            ).astype(BF16)

    def memory_copy(j):
        rows = rows_of(j, 2 * BLOCK)
        return partner_copy(
            mix_memory.at[1, rows, pl.ds(0, width)],
            mix_memory.at[0, rows, pl.ds(width, width)],
            mem_send.at[j],
            mem_recv.at[j],
        )

    early = n_out // 2

    @pl.loop(0, n_out)
    def _(j):
        slot = jnp.where(j < early, 1, 0)
        side = jnp.where(j < early, other, me)
        pair = lax.rem(j, early)
        cols = rows_of(j, out_cols)
        acc[:, cols] = dot(mix_conv[0], out_c[:, cols])
        for i in range(2):
            finish_block(side, slot, 2 * pair + i)

        @pl.when(j < early)
        def _():
            memory_copy(j).start()

    for j in range(early):
        memory_copy(j).wait_recv()

    @pl.loop(0, n_out)
    def _(j):
        cols = rows_of(j, out_cols)
        layer_out[:, cols] = (acc[:, cols] + dot(mix_memory[0], out_m[:, cols])).astype(BF16)

    for c in range(n_half):
        norm_copy(c).wait_send()
    for c in outw_copies:
        c.wait_send()
    conv_copy.wait_send()
    for j in range(early):
        memory_copy(j).wait_send()

    @pl.when(place + 1 < n_sp)
    def _():
        rim_copy.wait_send()
        for k in range(BATCHES):
            for c in state_copies(k):
                c.wait_send()


def local(
    tokens,
    norm_gain,
    w_query,
    w_key,
    w_value,
    w_outgate,
    w_gatein,
    w_gateout,
    w_convin,
    w_igate,
    w_fgate,
    input_bias,
    forget_bias,
    forget_extra,
    init_memory,
    head_gain,
    conv_taps,
    out_memory,
    out_conv,
):
    heads, dh = init_memory.shape[1], init_memory.shape[2]
    half, features = tokens.shape[1], tokens.shape[2]
    rows = forget_extra.shape[1]
    width = w_query.shape[1]
    nblocks = rows // BLOCK
    n_half = half // BLOCK
    all_heads = w_igate.shape[1]
    n_sp = lax.axis_size("sp")
    hbm = pl.BlockSpec(memory_space=pl.ANY)
    dma = pltpu.SemaphoreType.DMA
    out = pl.pallas_call(
        functools.partial(kernel, n_sp),
        name="layer",
        out_shape=pltpu.VMEM((half, features), BF16),
        in_specs=[hbm] * 19,
        out_specs=pl.BlockSpec(memory_space=pltpu.VMEM),
        scratch_shapes=[
            pltpu.VMEM((half, features), BF16),
            pltpu.VMEM((features // BLOCK, BLOCK), BF16),
            pltpu.VMEM((1, features), F32),
            pltpu.VMEM((all_heads, dh), BF16),
            pltpu.VMEM((all_heads, dh), F32),
            pltpu.VMEM((all_heads, features), BF16),
            pltpu.VMEM((all_heads, features), BF16),
            pltpu.VMEM((features, BLOCK), BF16),
            pltpu.SMEM((2, all_heads), F32),
            pltpu.VMEM((heads, rows), F32),
            pltpu.VMEM((heads, dh, dh), F32),
            pltpu.VMEM(conv_taps.shape, BF16),
            pltpu.VMEM((rows, features), BF16),
            pltpu.VMEM((7, features, width), BF16),
            pltpu.VMEM((2 * width, features), BF16),
            pltpu.VMEM((2 * width, features), BF16),
            pltpu.VMEM((rows, width), BF16),
            pltpu.VMEM((rows, width), BF16),
            pltpu.VMEM((rows, width), BF16),
            pltpu.VMEM((2, rows, width), BF16),
            pltpu.VMEM((rows, width), BF16),
            pltpu.VMEM((rows, width), BF16),
            pltpu.VMEM((rows, BLOCK), F32),
            pltpu.VMEM((nblocks, 2 * PAD, BLOCK), F32),
            pltpu.VMEM((nblocks, BLOCK, BLOCK), F32),
            pltpu.VMEM((nblocks, PAD, BLOCK), F32),
            pltpu.VMEM((nblocks, PAD, BLOCK), F32),
            pltpu.VMEM((nblocks, heads, dh, dh), BF16),
            pltpu.VMEM((nblocks, BLOCK, BLOCK), F32),
            pltpu.VMEM((2, heads, dh, dh), F32),
            pltpu.VMEM((2, PAD, BLOCK), F32),
            pltpu.VMEM((2, PAD, BLOCK), F32),
            pltpu.VMEM((4, PAD, BLOCK), F32),
            pltpu.VMEM((2, heads, dh, dh), BF16),
            pltpu.VMEM((2, PAD, BLOCK), F32),
            pltpu.VMEM((2, BLOCK, BLOCK), F32),
            pltpu.VMEM((heads, dh, dh), BF16),
            pltpu.VMEM((PAD, BLOCK), F32),
            pltpu.VMEM((rows, width), F32),
            pltpu.VMEM((nblocks, BLOCK, BLOCK), F32),
            pltpu.VMEM((RIM + rows, width), BF16),
            pltpu.VMEM((RIM, width), BF16),
            pltpu.VMEM((RIM, width), BF16),
            pltpu.VMEM((2, half, 2 * width), BF16),
            pltpu.VMEM((2, half, 2 * width), BF16),
            pltpu.VMEM((half, features), F32),
            dma((n_half,)),
            dma((9,)),
            dma((9,)),
            dma((n_half,)),
            dma((n_half,)),
            dma((2,)),
            dma((2,)),
            dma((BATCHES + 1,)),
            dma((BATCHES + 1,)),
            dma((2,)),
            dma((2,)),
            dma((n_half // 2,)),
            dma((n_half // 2,)),
        ],
        compiler_params=pltpu.CompilerParams(
            collective_id=0, has_side_effects=True, vmem_limit_bytes=60 * 1024 * 1024
        ),
    )(
        tokens[0],
        norm_gain.reshape(-1, BLOCK),
        w_key,
        w_value,
        w_query,
        w_gatein,
        w_convin,
        w_gateout,
        w_outgate,
        jnp.transpose(w_igate),
        jnp.transpose(w_fgate),
        input_bias,
        forget_bias,
        jnp.transpose(forget_extra[0]),
        init_memory[0],
        head_gain.reshape(-1, dh),
        conv_taps,
        out_memory,
        out_conv,
    )
    return out[None]


def solution(mesh):
    return jax.shard_map(
        local,
        mesh=mesh,
        in_specs=(
            P("fs", ("sp", "tp"), None),
            P(),
            P(None, "tp"),
            P(None, "tp"),
            P(None, "tp"),
            P(None, "tp"),
            P(None, "tp"),
            P(None, "tp"),
            P(None, "tp"),
            P(),
            P(),
            P(),
            P(),
            P("fs", "sp", "tp"),
            P("fs", "tp", None, None),
            P(),
            P(),
            P("tp", None),
            P("tp", None),
        ),
        out_specs=P("fs", ("sp", "tp"), None),
        check_vma=False,
    )
```

time: 48.4 us -> 36.6 us (0.76); the launches traced: 47.5 us -> 36.2 us
  Pallas kernels: 46.2 us -> 34.9 us
    pallas_call x1, Pallas kernels: 46.2 us -> 34.9 us  [local(): pl.pallas_call(functools.partial(kernel, n_sp), name='layer', out_shape=p...]
where the time goes in v1:
time: 36.6 us; the launch traced here: 36.2 us
  Pallas kernels  34.9 us (95%)
  local copies, waits for them, and re-layouts  1.32 us (4%)
    pallas_call x1, Pallas kernels, local(): pl.pallas_call(functools.partial(kernel, n_sp), name='layer', out_shape=p...  34.9 us
    unnamed x1, local copies, waits for them, and re-layouts  1.32 us

profile of v1, /device:TPU:10, one launch (start us, length us, event | category | flops | bytes accessed | tf_op | source)
XLA Modules:
  0.0 36.2 jit_solution(14365762643387355553)
XLA Ops:
  0.0 34.9 %layer.1 = bf16[512,2048]{1,0:T(8,128)(2,1)S(1)} custom-call(bf16[512,2048]{1,0:T(8,128)(2,1)} %bitcast.11, bf16[16,128]{1,0:T(8,128)(2,1)} %bitcast.16, bf16[2048,512]{1,0:T(8,128)(2,1)} %w_key.1, bf16[2048,512]{1,0:T(8,128)(2,1)} %w_value.1, bf16[2048,512]{1,0:T(8,128)(2,1)} %w_query.1, bf16[2048,512]{1,0:T(8,128)(2,1)} %w_gatein.1, ...), custom_call_target="tpu_custom_call" | custom-call | tf_op jit(solution)/shard_map/layer/pallas_call | solution.py:639
  34.9 1.3 %copy.21 = bf16[1,512,2048]{2,1,0:T(8,128)(2,1)} copy(bf16[1,512,2048]{2,1,0:T(8,128)(2,1)S(1)} %bitcast.10) | data formatting | bytes 4194304

commit v2 on v1

--- a/solution.py
+++ b/solution.py
@@ -14,9 +14,10 @@
 F32 = jnp.float32
 BF16 = jnp.bfloat16
 PAD = 8
-RIM = 16
+RIM = 8
 NORM_ROWS = 64
 BATCHES = 2
+PARTS = 2
 
 KEY, VALUE, QUERY, GATE_IN, CONV_IN, GATE_OUT, OUT_GATE = range(7)
 
@@ -115,8 +116,6 @@
     nblocks = total_rows // BLOCK
     key_factor = dh ** (-0.5)
     out_width = layer_out.shape[1]
-    n_out = n_half
-    out_cols = out_width // n_out
     group = heads // BATCHES
 
     barrier = pltpu.get_barrier_semaphore()
@@ -190,15 +189,20 @@
         gain_row[:, j * BLOCK : (j + 1) * BLOCK] = gain_in[j : j + 1].astype(F32)
 
     def normalize(c):
-        @pl.loop(0, BLOCK // NORM_ROWS)
-        def _(part):
+        for part in range(BLOCK // NORM_ROWS):
             start = c * BLOCK + part * NORM_ROWS
-            x = tok[pl.ds(pl.multiple_of(start, NORM_ROWS), NORM_ROWS), :].astype(F32)
+            x = tok[pl.ds(start, NORM_ROWS), :].astype(F32)
             scale = lax.rsqrt(jnp.mean(x * x, axis=-1, keepdims=True) + EPSILON)
             y = (x * scale) * gain_row[...]
             normed[pl.ds(pl.multiple_of(me * half + start, NORM_ROWS), NORM_ROWS), :] = y.astype(
                 BF16
             )
+
+    def gate_dot(c):
+        rows = pl.ds(pl.multiple_of(me * half + c * BLOCK, BLOCK), BLOCK)
+        gate_pre[rows, :] = jnp.dot(
+            normed[rows, :], gate_w[...], preferred_element_type=F32
+        )
 
     first_weights = 3
     smalls[1].wait()
@@ -216,6 +220,8 @@
         tok_copies[c].wait()
         if c < first_weights:
             w_copies[c].start()
+        if c > 0:
+            gate_dot(c - 1)
         normalize(c)
     for c in w_copies[min(first_weights, n_half) :]:
         c.start()
@@ -251,10 +257,12 @@
     def dot(a, b):
         return jnp.dot(a, b, preferred_element_type=F32)
 
-    def project(target, slot, rows):
+    def project(target, slot, index, part):
+        size = half // PARTS
+        rows = rows_of(index * PARTS + part, size)
         target[rows, :] = dot(normed[rows, :], weights[slot]).astype(BF16)
 
-    def gate_math(index):
+    def gate_sums(index):
         forget_rows, in_rows = [], []
         for j in range(n_half):
             span = rows_of(index * n_half + j, BLOCK)
@@ -269,7 +277,9 @@
             precision=lax.Precision.HIGHEST,
             preferred_element_type=F32,
         )
-        all_in = jnp.concatenate(in_rows, axis=0)
+        return all_cumulative, jnp.concatenate(in_rows, axis=0)
+
+    def gate_logs(index, all_cumulative, all_in):
         all_total = jnp.broadcast_to(all_cumulative[:, BLOCK - 1 : BLOCK], all_in.shape)
         exponent = all_total - all_cumulative + all_in
         all_peak = jnp.broadcast_to(jnp.max(exponent, axis=1, keepdims=True), all_in.shape)
@@ -286,7 +296,25 @@
                 jnp.concatenate([all_cumulative[span], key_weight[span], filler], axis=0)
             )
 
-    def half_state(index):
+    def block_terms(index):
+        terms = []
+        for h in range(heads):
+            for j in range(n_half):
+                b = index * n_half + j
+                rows = rows_of(b, BLOCK)
+                k = k_rows[rows, head_cols(h)].astype(F32)
+                wk = (col_log[b, :, PAD + h : PAD + h + 1] * k).astype(BF16)
+                terms.append(
+                    lax.dot_general(
+                        wk,
+                        v_rows[rows, head_cols(h)],
+                        (((0,), (0,)), ((), ())),
+                        preferred_element_type=F32,
+                    )
+                )
+        return terms
+
+    def half_state(index, terms):
         log = jnp.full((PAD, BLOCK), LOWEST_LOG, F32)
         total = jnp.zeros((PAD, BLOCK), F32)
         filler = jnp.zeros((BLOCK - 2 * PAD, BLOCK), F32)
@@ -305,60 +333,58 @@
         for h in range(heads):
             state = jnp.zeros((dh, dh), F32)
             for j in range(n_half):
-                b = index * n_half + j
-                rows = rows_of(b, BLOCK)
-                prefix[b, h] = state.astype(BF16)
-                k = k_rows[rows, head_cols(h)].astype(F32)
-                wk = (col_log[b, :, PAD + h : PAD + h + 1] * k).astype(BF16)
-                term = lax.dot_general(
-                    wk,
-                    v_rows[rows, head_cols(h)],
-                    (((0,), (0,)), ((), ())),
-                    preferred_element_type=F32,
+                prefix[index * n_half + j, h] = state.astype(BF16)
+                state = (
+                    keeps[j][h : h + 1] * state + adds[j][h : h + 1] * terms[h * n_half + j]
                 )
-                state = keeps[j][h : h + 1] * state + adds[j][h : h + 1] * term
             half_sum[index, h] = state
 
-    own_rows = rows_of(me, half)
-    gate_pre[own_rows, :] = dot(normed[own_rows, :], gate_w[...])
+    def keys(index):
+        for p in range(PARTS):
+            project(k_rows, KEY, index, p)
+
+    def values_queries(index):
+        project(v_rows, VALUE, index, 0)
+        sums = gate_sums(index)
+        project(v_rows, VALUE, index, 1)
+        gate_logs(index, *sums)
+        project(q_rows, QUERY, index, 0)
+        terms = block_terms(index)
+        project(q_rows, QUERY, index, 1)
+        half_state(index, terms)
+
+    once = jnp.minimum(place + 1, 1)
+
+    def region(body):
+        pl.loop(0, once)(lambda _: body())
+
     pl.semaphore_wait(barrier, jnp.where(place + 1 < n_sp, 2, 1))
     for c in range(n_half):
         norm_copy(c).start()
-
-    @pl.loop(0, 2)
-    def _(step):
-        index = lax.rem(me + step, 2)
-        rows = rows_of(index, half)
-
-        @pl.when(step == 0)
-        def _():
-            w_copies[KEY].wait()
-
-        @pl.when(step == 1)
-        def _():
-            for c in range(n_half):
-                norm_copy(c).wait_recv()
-            gate_pre[rows, :] = dot(normed[rows, :], gate_w[...])
-
-        project(k_rows, KEY, rows)
-
-        @pl.when(step == 0)
-        def _():
-            w_copies[VALUE].wait()
-            for c in out_copies:
-                c.start()
-            for c in outw_copies:
-                c.start()
-
-        project(v_rows, VALUE, rows)
-        gate_math(index)
-
-        @pl.when(step == 0)
-        def _():
-            w_copies[QUERY].wait()
-
-        project(q_rows, QUERY, rows)
-        half_state(index)
+    w_copies[KEY].wait()
+    @region
+    def _():
+        gate_dot(n_half - 1)
+        keys(me)
+
+    w_copies[VALUE].wait()
+    w_copies[QUERY].wait()
+    for c in out_copies:
+        c.start()
+    for c in outw_copies:
+        c.start()
+    @region
+    def _():
+        values_queries(me)
+
+    for c in range(n_half):
+        norm_copy(c).wait_recv()
+    @region
+    def _():
+        other_rows = rows_of(other, half)
+        gate_pre[other_rows, :] = dot(normed[other_rows, :], gate_w[...])
+        keys(other)
+        values_queries(other)
 
     for c in w_copies[GATE_IN:]:
         c.wait()
@@ -416,33 +442,42 @@
 
     def relays(g):
         for k in range(BATCHES):
-            due = jnp.where(place == 0, 0, jnp.minimum(2 * place + k, n_main))
+            due = jnp.where(place == 0, 0, jnp.minimum(2 * place + 1 + k, n_main))
 
             @pl.when(due == g)
             def _(k=k):
                 relay(k)
 
-    def read_block(b):
+    def read_scores(b):
+        rows = rows_of(b, BLOCK)
+        return [
+            lax.dot_general(
+                q_rows[rows, head_cols(h)],
+                k_rows[rows, head_cols(h)],
+                (((1,), (1,)), ((), ())),
+                preferred_element_type=F32,
+            )
+            for h in range(heads)
+        ]
+
+    def read_values(b, scores):
         rows = rows_of(b, BLOCK)
         columns = col_log[b]
         carried_all = columns + prefix_cols[b]
         tops = jnp.zeros((BLOCK, BLOCK), F32)
         for h in range(heads):
-            q = q_rows[rows, head_cols(h)]
-            k = k_rows[rows, head_cols(h)]
-            scores = lax.dot_general(
-                q, k, (((1,), (1,)), ((), ())), preferred_element_type=F32
-            )
-            carried = dot(q, prefix[b, h])
             pair = (columns[:, h : h + 1] - row_log[b, h : h + 1]) + row_log[
                 b, PAD + h : PAD + h + 1
             ]
             pair = jnp.where(causal, pair, -jnp.inf)
             carried_log = carried_all[:, h : h + 1]
             top = jnp.maximum(carried_log, jnp.max(pair, axis=1, keepdims=True))
-            weighted = (jnp.exp(pair - top) * (scores * key_factor)).astype(BF16)
-            local_out[rows, head_cols(h)] = jnp.exp(carried_log - top) * carried + dot(
-                weighted, v_rows[rows, head_cols(h)]
+            weighted = (jnp.exp(pair - top) * (scores[h] * key_factor)).astype(BF16)
+            q = q_rows[rows, head_cols(h)].astype(F32)
+            carried = (jnp.exp(carried_log - top) * q).astype(BF16)
+            local_out[rows, head_cols(h)] = dot(
+                jnp.concatenate([weighted, carried], axis=1),
+                jnp.concatenate([v_rows[rows, head_cols(h)], prefix[b, h]], axis=0),
             )
             tops = jnp.where(col_i == h, top, tops)
         local_top[b] = tops
@@ -451,8 +486,25 @@
     taps = conv_taps[:, taps_cols].astype(F32)
     tap_count = conv_taps.shape[0]
 
-    def product(rows):
-        return (conv_pair[0, rows, :].astype(F32) * conv_pair[1, rows, :].astype(F32)).astype(BF16)
+    def product(rows, cols):
+        return conv_pair[0, rows, cols].astype(F32) * conv_pair[1, rows, cols].astype(F32)
+
+    def products(b):
+        target = pl.ds(pl.multiple_of(RIM + b * BLOCK, RIM), BLOCK)
+        for h in range(heads):
+            conv_rows[h, target, :] = product(rows_of(b, BLOCK), head_cols(h))
+
+    def convolve(b, slot, j):
+        for h in range(heads):
+            cols = head_cols(h)
+            mixed = None
+            for t in range(tap_count):
+                x = conv_rows[h, pl.ds(b * BLOCK + (RIM - tap_count + 1 + t), BLOCK), :]
+                y = x * taps[t : t + 1, cols]
+                mixed = y if mixed is None else mixed + y
+            mix_conv[slot, pl.ds(j * BLOCK, BLOCK), cols] = (
+                go_rows[rows_of(b, BLOCK), cols].astype(F32) * mixed
+            ).astype(BF16)
 
     split = n_main // 2
 
@@ -460,10 +512,14 @@
     def _(g):
         relays(g)
         slot = lax.div(g, n_half // 2)
-        project(conv_pair.at[slot], GATE_IN + slot, rows_of(lax.rem(g, 2), half))
-        read_block(g)
-
-    rim_out[...] = product(pl.ds(total_rows - RIM, RIM))
+        index = lax.rem(g, 2)
+        scores = read_scores(g)
+        project(conv_pair.at[slot], GATE_IN + slot, index, 0)
+        read_values(g, scores)
+        project(conv_pair.at[slot], GATE_IN + slot, index, 1)
+
+    for h in range(heads):
+        rim_out[h] = product(pl.ds(total_rows - 2 * RIM, 2 * RIM), head_cols(h))[RIM:]
     rim_copy = pltpu.make_async_remote_copy(
         src_ref=rim_out,
         dst_ref=rim,
@@ -481,21 +537,21 @@
     def _(g):
         relays(g)
         index = g - split
+        scores = read_scores(g)
+        project(go_rows, GATE_OUT, index, 0)
+        read_values(g, scores)
         for j in range(n_half):
-            b = index * n_half + j
-            target = pl.ds(pl.multiple_of(RIM + b * BLOCK, RIM), BLOCK)
-            conv_rows[target, :] = product(rows_of(b, BLOCK))
-        project(go_rows, GATE_OUT, rows_of(index, half))
-        read_block(g)
+            products(index * n_half + j)
+        project(go_rows, GATE_OUT, index, 1)
 
     @pl.when(place > 0)
     def _():
         rim_copy.wait_recv()
-        conv_rows[0:RIM, :] = rim[...]
+        conv_rows[:, 0:RIM, :] = rim[...]
 
     @pl.when(place == 0)
     def _():
-        conv_rows[0:RIM, :] = jnp.zeros((RIM, width), BF16)
+        conv_rows[:, 0:RIM, :] = jnp.zeros((heads, RIM, dh), F32)
 
     conv_copy = partner_copy(
         mix_conv.at[1, :, pl.ds(0, width)],
@@ -509,20 +565,12 @@
         relays(g)
         turn = g - (split + 2)
         side = jnp.where(turn == 0, other, me)
+        scores = read_scores(g)
+        project(og_rows, OUT_GATE, turn, 0)
+        read_values(g, scores)
         for j in range(n_half):
-            b = side * n_half + j
-            x = conv_rows[pl.ds(pl.multiple_of(b * BLOCK, RIM), BLOCK + RIM), :].astype(F32)
-            mixed = None
-            for t in range(tap_count):
-                back = tap_count - 1 - t
-                y = x if back == 0 else pltpu.roll(x, back, 0)
-                y = y[RIM:] * taps[t : t + 1]
-                mixed = y if mixed is None else mixed + y
-            mix_conv[1 - turn, pl.ds(j * BLOCK, BLOCK), pl.ds(0, width)] = (
-                go_rows[rows_of(b, BLOCK), :].astype(F32) * mixed
-            ).astype(BF16)
-        project(og_rows, OUT_GATE, rows_of(turn, half))
-        read_block(g)
+            convolve(side * n_half + j, 1 - turn, j)
+        project(og_rows, OUT_GATE, turn, 1)
 
         @pl.when(turn == 0)
         def _():
@@ -535,7 +583,11 @@
         c.wait_recv()
     conv_copy.wait_recv()
 
-    def finish_block(side, slot, j):
+    def finish_dots(side, j):
+        rows = rows_of(side * n_half + j, BLOCK)
+        return [dot(q_rows[rows, head_cols(h)], carry[side, h]) for h in range(heads)]
+
+    def finish_block(side, slot, j, carried):
         b = side * n_half + j
         rows = rows_of(b, BLOCK)
         local = local_top[b]
@@ -546,8 +598,7 @@
         local_factor = jnp.exp(local - top)
         carried_factor = jnp.exp(carried_all - top)
         for h in range(heads):
-            q = q_rows[rows, head_cols(h)]
-            out = carried_factor[:, h : h + 1] * dot(q, carry[side, h]) + local_factor[
+            out = carried_factor[:, h : h + 1] * carried[h] + local_factor[
                 :, h : h + 1
             ] * local_out[rows, head_cols(h)]
             out = out * lax.rsqrt(jnp.mean(out * out, axis=1, keepdims=True) + EPSILON)
@@ -557,7 +608,7 @@
             ).astype(BF16)
 
     def memory_copy(j):
-        rows = rows_of(j, 2 * BLOCK)
+        rows = rows_of(j, BLOCK)
         return partner_copy(
             mix_memory.at[1, rows, pl.ds(0, width)],
             mix_memory.at[0, rows, pl.ds(width, width)],
@@ -565,36 +616,44 @@
             mem_recv.at[j],
         )
 
-    early = n_out // 2
-
-    @pl.loop(0, n_out)
-    def _(j):
-        slot = jnp.where(j < early, 1, 0)
-        side = jnp.where(j < early, other, me)
-        pair = lax.rem(j, early)
-        cols = rows_of(j, out_cols)
-        acc[:, cols] = dot(mix_conv[0], out_c[:, cols])
-        for i in range(2):
-            finish_block(side, slot, 2 * pair + i)
-
-        @pl.when(j < early)
+    wide = out_width // 2
+
+    @pl.loop(0, 2)
+    def _(turn):
+        side = jnp.where(turn == 0, other, me)
+        cols = rows_of(turn, wide)
+        size = half // PARTS
+        carried = [finish_dots(side, j) for j in range(n_half)]
+        for p in range(PARTS):
+            rows = slice(p * size, (p + 1) * size)
+            acc[rows, cols] = dot(mix_conv[0, rows, :], out_c[:, cols])
+            for j in range(p * n_half // PARTS, (p + 1) * n_half // PARTS):
+                finish_block(side, 1 - turn, j, carried[j])
+
+        @pl.when(turn == 0)
         def _():
-            memory_copy(j).start()
-
-    for j in range(early):
+            for j in range(n_half):
+                memory_copy(j).start()
+
+    @region
+    def _():
+        acc[...] += dot(mix_memory[0, :, 0:width], out_m[0:width, :])
+
+    for j in range(n_half):
         memory_copy(j).wait_recv()
 
-    @pl.loop(0, n_out)
-    def _(j):
-        cols = rows_of(j, out_cols)
-        layer_out[:, cols] = (acc[:, cols] + dot(mix_memory[0], out_m[:, cols])).astype(BF16)
+    @region
+    def _():
+        layer_out[...] = (
+            acc[...] + dot(mix_memory[0, :, width:], out_m[pl.ds(width, width), :])
+        ).astype(BF16)
 
     for c in range(n_half):
         norm_copy(c).wait_send()
     for c in outw_copies:
         c.wait_send()
     conv_copy.wait_send()
-    for j in range(early):
+    for j in range(n_half):
         memory_copy(j).wait_send()
 
     @pl.when(place + 1 < n_sp)
@@ -683,9 +742,9 @@
             pltpu.VMEM((PAD, BLOCK), F32),
             pltpu.VMEM((rows, width), F32),
             pltpu.VMEM((nblocks, BLOCK, BLOCK), F32),
-            pltpu.VMEM((RIM + rows, width), BF16),
-            pltpu.VMEM((RIM, width), BF16),
-            pltpu.VMEM((RIM, width), BF16),
+            pltpu.VMEM((heads, RIM + rows, dh), F32),
+            pltpu.VMEM((heads, RIM, dh), F32),
+            pltpu.VMEM((heads, RIM, dh), F32),
             pltpu.VMEM((2, half, 2 * width), BF16),
             pltpu.VMEM((2, half, 2 * width), BF16),
             pltpu.VMEM((half, features), F32),
@@ -700,8 +759,8 @@
             dma((BATCHES + 1,)),
             dma((2,)),
             dma((2,)),
-            dma((n_half // 2,)),
-            dma((n_half // 2,)),
+            dma((n_half,)),
+            dma((n_half,)),
         ],
         compiler_params=pltpu.CompilerParams(
             collective_id=0, has_side_effects=True, vmem_limit_bytes=60 * 1024 * 1024

time: 36.6 us -> 34.1 us (0.932)
  Pallas kernels: 34.9 us -> 32.3 us
    pallas_call x1, Pallas kernels: 34.9 us -> 32.3 us  [local(): pl.pallas_call(functools.partial(kernel, n_sp), name='layer', out_shape=p...]
where the time goes in v2:
time: 34.1 us; the launch traced here: 33.6 us
  Pallas kernels  32.3 us (95%)
  local copies, waits for them, and re-layouts  1.32 us (4%)
    pallas_call x1, Pallas kernels, local(): pl.pallas_call(functools.partial(kernel, n_sp), name='layer', out_shape=p...  32.3 us
    unnamed x1, local copies, waits for them, and re-layouts  1.32 us

profile of v2, /device:TPU:10, one launch (start us, length us, event | category | flops | bytes accessed | tf_op | source)
XLA Modules:
  0.0 33.6 jit_solution(9746536791391848640)
XLA Ops:
  0.0 32.3 %layer.1 = bf16[512,2048]{1,0:T(8,128)(2,1)S(1)} custom-call(bf16[512,2048]{1,0:T(8,128)(2,1)} %bitcast.11, bf16[16,128]{1,0:T(8,128)(2,1)} %bitcast.16, bf16[2048,512]{1,0:T(8,128)(2,1)} %w_key.1, bf16[2048,512]{1,0:T(8,128)(2,1)} %w_value.1, bf16[2048,512]{1,0:T(8,128)(2,1)} %w_query.1, bf16[2048,512]{1,0:T(8,128)(2,1)} %w_gatein.1, ...), custom_call_target="tpu_custom_call" | custom-call | tf_op jit(solution)/shard_map/layer/pallas_call | solution.py:698
  32.3 1.3 %copy.21 = bf16[1,512,2048]{2,1,0:T(8,128)(2,1)} copy(bf16[1,512,2048]{2,1,0:T(8,128)(2,1)S(1)} %bitcast.10) | data formatting | bytes 4194304

commit v3 on v2

--- a/solution.py
+++ b/solution.py
@@ -73,6 +73,7 @@
     block_peak,
     prefix,
     prefix_cols,
+    total_cols,
     half_sum,
     half_log,
     half_total,
@@ -99,6 +100,7 @@
     outw_recv,
     state_send,
     state_recv,
+    ready,
     rim_sem,
     conv_sem,
     mem_send,
@@ -117,13 +119,17 @@
     key_factor = dh ** (-0.5)
     out_width = layer_out.shape[1]
     group = heads // BATCHES
+    chunks, piece = out_c.shape[0], out_c.shape[2]
 
     barrier = pltpu.get_barrier_semaphore()
     pl.semaphore_signal(barrier, inc=1, device_id={"tp": other}, device_id_type=MESH)
 
-    @pl.when(place > 0)
-    def _():
-        pl.semaphore_signal(barrier, inc=1, device_id={"sp": place - 1}, device_id_type=MESH)
+    @pl.when(place + 1 < n_sp)
+    def _():
+        pl.semaphore_signal(barrier, inc=1, device_id={"sp": place + 1}, device_id_type=MESH)
+
+    def head_cols(h):
+        return slice(h * dh, (h + 1) * dh)
 
     def rows_of(index, size):
         return pl.ds(pl.multiple_of(index * size, size), size)
@@ -156,7 +162,11 @@
     ]
     out_copies = [
         pltpu.make_async_copy(out_memory, out_m.at[pl.ds(0, width)], weight_sem.at[7]),
-        pltpu.make_async_copy(out_conv, out_c.at[pl.ds(0, width)], weight_sem.at[8]),
+    ] + [
+        pltpu.make_async_copy(
+            out_conv.at[:, pl.ds(c * piece, piece)], out_c.at[c, pl.ds(0, width)], weight_sem.at[8 + c]
+        )
+        for c in range(chunks)
     ]
 
     def partner_copy(src, dst, send_sem, recv_sem):
@@ -174,8 +184,17 @@
         return partner_copy(normed.at[rows], normed.at[rows], norm_send.at[c], norm_recv.at[c])
 
     outw_copies = [
-        partner_copy(src, dst.at[pl.ds(width, width)], outw_send.at[i], outw_recv.at[i])
-        for i, (src, dst) in enumerate(((out_conv, out_c), (out_memory, out_m)))
+        partner_copy(
+            out_conv.at[:, pl.ds(c * piece, piece)],
+            out_c.at[c, pl.ds(width, width)],
+            outw_send.at[c],
+            outw_recv.at[c],
+        )
+        for c in range(chunks)
+    ] + [
+        partner_copy(
+            out_memory, out_m.at[pl.ds(width, width)], outw_send.at[chunks], outw_recv.at[chunks]
+        )
     ]
 
     smalls[0].start()
@@ -185,6 +204,7 @@
         c.start()
 
     smalls[0].wait()
+    w_copies[0].start()
     for j in range(norm_gain.shape[0]):
         gain_row[:, j * BLOCK : (j + 1) * BLOCK] = gain_in[j : j + 1].astype(F32)
 
@@ -218,12 +238,21 @@
     gate_w[...] = jnp.transpose(gates)
     for c in range(n_half):
         tok_copies[c].wait()
-        if c < first_weights:
-            w_copies[c].start()
+        if c + 1 < first_weights:
+            w_copies[c + 1].start()
         if c > 0:
             gate_dot(c - 1)
         normalize(c)
-    for c in w_copies[min(first_weights, n_half) :]:
+        if c == 0:
+            pl.semaphore_wait(barrier, jnp.where(place > 0, 2, 1))
+
+            @pl.when(place > 0)
+            def _():
+                pl.semaphore_signal(
+                    ready, inc=1, device_id={"sp": place - 1}, device_id_type=MESH
+                )
+        norm_copy(c).start()
+    for c in w_copies[first_weights:]:
         c.start()
 
     for c in smalls[3:]:
@@ -240,9 +269,6 @@
     col_i = lax.broadcasted_iota(jnp.int32, (BLOCK, BLOCK), 1)
     upper = jnp.where(row_i <= col_i, 1.0, 0.0).astype(F32)
     causal = col_i <= row_i
-
-    def head_cols(h):
-        return slice(h * dh, (h + 1) * dh)
 
     first_head = me * heads
     to_front = lax.rem(PAD - first_head, PAD)
@@ -257,9 +283,9 @@
     def dot(a, b):
         return jnp.dot(a, b, preferred_element_type=F32)
 
-    def project(target, slot, index, part):
-        size = half // PARTS
-        rows = rows_of(index * PARTS + part, size)
+    def project(target, slot, index, part, parts=PARTS):
+        size = half // parts
+        rows = rows_of(index * parts + part, size)
         target[rows, :] = dot(normed[rows, :], weights[slot]).astype(BF16)
 
     def gate_sums(index):
@@ -317,11 +343,12 @@
     def half_state(index, terms):
         log = jnp.full((PAD, BLOCK), LOWEST_LOG, F32)
         total = jnp.zeros((PAD, BLOCK), F32)
-        filler = jnp.zeros((BLOCK - 2 * PAD, BLOCK), F32)
+        filler = jnp.zeros((BLOCK - PAD, BLOCK), F32)
         keeps, adds = [], []
         for j in range(n_half):
             b = index * n_half + j
-            prefix_cols[b] = jnp.transpose(jnp.concatenate([log, total, filler], axis=0))
+            prefix_cols[b] = jnp.transpose(jnp.concatenate([log, filler], axis=0))
+            total_cols[b] = jnp.transpose(jnp.concatenate([total, filler], axis=0))
             now, peak = block_sum[b], block_peak[b]
             merged = jnp.maximum(now + log, peak)
             keeps.append(jnp.exp(now + log - merged))
@@ -358,9 +385,6 @@
     def region(body):
         pl.loop(0, once)(lambda _: body())
 
-    pl.semaphore_wait(barrier, jnp.where(place + 1 < n_sp, 2, 1))
-    for c in range(n_half):
-        norm_copy(c).start()
     w_copies[KEY].wait()
     @region
     def _():
@@ -442,7 +466,8 @@
 
     def relays(g):
         for k in range(BATCHES):
-            due = jnp.where(place == 0, 0, jnp.minimum(2 * place + 1 + k, n_main))
+            due = jnp.where(place == 1, 2 + 2 * k, jnp.where(place == 2, 5 + k, n_main))
+            due = jnp.where(place == 0, 0, due)
 
             @pl.when(due == g)
             def _(k=k):
@@ -460,12 +485,11 @@
             for h in range(heads)
         ]
 
-    def read_values(b, scores):
+    def read_values(b, scores, tops, head_range):
         rows = rows_of(b, BLOCK)
         columns = col_log[b]
         carried_all = columns + prefix_cols[b]
-        tops = jnp.zeros((BLOCK, BLOCK), F32)
-        for h in range(heads):
+        for h in head_range:
             pair = (columns[:, h : h + 1] - row_log[b, h : h + 1]) + row_log[
                 b, PAD + h : PAD + h + 1
             ]
@@ -480,7 +504,26 @@
                 jnp.concatenate([v_rows[rows, head_cols(h)], prefix[b, h]], axis=0),
             )
             tops = jnp.where(col_i == h, top, tops)
-        local_top[b] = tops
+        return tops
+
+    no_tops = jnp.zeros((BLOCK, BLOCK), F32)
+
+    def unit(target, slot, index, reads, extras):
+        scores = [read_scores(b) for b in reads]
+        parts = max(len(extras), PARTS)
+        tops = [no_tops] * len(reads)
+        share = heads // PARTS
+        for p in range(parts):
+            project(target, slot, index, p, parts)
+            if p < PARTS:
+                for i, b in enumerate(reads):
+                    tops[i] = read_values(
+                        b, scores[i], tops[i], range(p * share, (p + 1) * share)
+                    )
+            if p < len(extras):
+                extras[p]()
+        for i, b in enumerate(reads):
+            local_top[b] = tops[i]
 
     taps_cols = pl.ds(pl.multiple_of(me * width, width), width)
     taps = conv_taps[:, taps_cols].astype(F32)
@@ -508,15 +551,22 @@
 
     split = n_main // 2
 
-    @pl.loop(0, split)
-    def _(g):
-        relays(g)
-        slot = lax.div(g, n_half // 2)
-        index = lax.rem(g, 2)
-        scores = read_scores(g)
-        project(conv_pair.at[slot], GATE_IN + slot, index, 0)
-        read_values(g, scores)
-        project(conv_pair.at[slot], GATE_IN + slot, index, 1)
+    late_reads = 2
+    early_reads = nblocks - late_reads
+    per_turn = early_reads // 2
+    gi_rows, ci_rows = conv_pair.at[0], conv_pair.at[1]
+
+    @pl.when(place + 1 < n_sp)
+    def _():
+        pl.semaphore_wait(ready, 1)
+
+    @pl.loop(0, 2)
+    def _(turn):
+        relays(2 * turn)
+        first = turn * per_turn
+        cut = (per_turn + 1) // 2
+        unit(gi_rows, GATE_IN, turn, [first + i for i in range(cut)], ())
+        unit(ci_rows, CONV_IN, turn, [first + i for i in range(cut, per_turn)], ())
 
     for h in range(heads):
         rim_out[h] = product(pl.ds(total_rows - 2 * RIM, 2 * RIM), head_cols(h))[RIM:]
@@ -537,12 +587,13 @@
     def _(g):
         relays(g)
         index = g - split
-        scores = read_scores(g)
-        project(go_rows, GATE_OUT, index, 0)
-        read_values(g, scores)
-        for j in range(n_half):
-            products(index * n_half + j)
-        project(go_rows, GATE_OUT, index, 1)
+        unit(
+            go_rows,
+            GATE_OUT,
+            index,
+            [early_reads + index],
+            [functools.partial(products, index * n_half + j) for j in range(n_half)],
+        )
 
     @pl.when(place > 0)
     def _():
@@ -565,12 +616,16 @@
         relays(g)
         turn = g - (split + 2)
         side = jnp.where(turn == 0, other, me)
-        scores = read_scores(g)
-        project(og_rows, OUT_GATE, turn, 0)
-        read_values(g, scores)
-        for j in range(n_half):
-            convolve(side * n_half + j, 1 - turn, j)
-        project(og_rows, OUT_GATE, turn, 1)
+        unit(
+            og_rows,
+            OUT_GATE,
+            turn,
+            (),
+            [
+                functools.partial(convolve, side * n_half + j, 1 - turn, j)
+                for j in range(n_half)
+            ],
+        )
 
         @pl.when(turn == 0)
         def _():
@@ -581,30 +636,30 @@
         c.wait()
     for c in outw_copies:
         c.wait_recv()
-    conv_copy.wait_recv()
-
-    def finish_dots(side, j):
+
+    def factors(side, j):
+        b = side * n_half + j
+        local = local_top[b]
+        carried_all = col_log[b] + total_cols[b] + carry_cols[side]
+        top = jnp.maximum(local, carried_all)
+        return jnp.exp(local - top), jnp.exp(carried_all - top)
+
+    def finish_heads(side, slot, j, group, carried, local_factor, carried_factor):
         rows = rows_of(side * n_half + j, BLOCK)
-        return [dot(q_rows[rows, head_cols(h)], carry[side, h]) for h in range(heads)]
-
-    def finish_block(side, slot, j, carried):
-        b = side * n_half + j
-        rows = rows_of(b, BLOCK)
-        local = local_top[b]
-        carried_all = (
-            col_log[b] + pltpu.roll(prefix_cols[b], BLOCK - PAD, 1) + carry_cols[side]
-        )
-        top = jnp.maximum(local, carried_all)
-        local_factor = jnp.exp(local - top)
-        carried_factor = jnp.exp(carried_all - top)
-        for h in range(heads):
-            out = carried_factor[:, h : h + 1] * carried[h] + local_factor[
-                :, h : h + 1
-            ] * local_out[rows, head_cols(h)]
-            out = out * lax.rsqrt(jnp.mean(out * out, axis=1, keepdims=True) + EPSILON)
-            gate = jax.nn.sigmoid(og_rows[rows, head_cols(h)].astype(F32))
+        outs = [
+            carried_factor[:, h : h + 1] * c
+            + local_factor[:, h : h + 1] * local_out[rows, head_cols(h)]
+            for h, c in zip(group, carried)
+        ]
+        means = [jnp.mean(out * out, axis=1, keepdims=True) for out in outs]
+        gates = [
+            head_rows[pl.ds(first_head + h, 1), :]
+            * jax.nn.sigmoid(og_rows[rows, head_cols(h)].astype(F32))
+            for h in group
+        ]
+        for h, out, mean, gate in zip(group, outs, means, gates):
             mix_memory[slot, rows_of(j, BLOCK), head_cols(h)] = (
-                out * head_rows[pl.ds(first_head + h, 1), :] * gate
+                out * lax.rsqrt(mean + EPSILON) * gate
             ).astype(BF16)
 
     def memory_copy(j):
@@ -616,19 +671,27 @@
             mem_recv.at[j],
         )
 
-    wide = out_width // 2
-
     @pl.loop(0, 2)
     def _(turn):
+        @pl.when(turn == 1)
+        def _():
+            conv_copy.wait_recv()
         side = jnp.where(turn == 0, other, me)
-        cols = rows_of(turn, wide)
-        size = half // PARTS
-        carried = [finish_dots(side, j) for j in range(n_half)]
-        for p in range(PARTS):
-            rows = slice(p * size, (p + 1) * size)
-            acc[rows, cols] = dot(mix_conv[0, rows, :], out_c[:, cols])
-            for j in range(p * n_half // PARTS, (p + 1) * n_half // PARTS):
-                finish_block(side, 1 - turn, j, carried[j])
+        share = heads // 2
+        part_cols = rows_of(turn, width)
+        in_chunks = chunks // 2
+        for j in range(n_half):
+            b_rows = rows_of(side * n_half + j, BLOCK)
+            rows = slice(j * BLOCK, (j + 1) * BLOCK)
+            mixed = factors(side, j)
+            for i in range(2):
+                group = range(i * share, (i + 1) * share)
+                carried = [dot(q_rows[b_rows, head_cols(h)], carry[side, h]) for h in group]
+                for c in range(i * in_chunks, (i + 1) * in_chunks):
+                    acc[turn, rows, c * piece : (c + 1) * piece] = dot(
+                        mix_conv[0, rows, part_cols], out_c[c, part_cols, :]
+                    )
+                finish_heads(side, 1 - turn, j, group, carried, *mixed)
 
         @pl.when(turn == 0)
         def _():
@@ -637,7 +700,7 @@
 
     @region
     def _():
-        acc[...] += dot(mix_memory[0, :, 0:width], out_m[0:width, :])
+        acc[0] = acc[0] + acc[1] + dot(mix_memory[0, :, 0:width], out_m[0:width, :])
 
     for j in range(n_half):
         memory_copy(j).wait_recv()
@@ -645,7 +708,7 @@
     @region
     def _():
         layer_out[...] = (
-            acc[...] + dot(mix_memory[0, :, width:], out_m[pl.ds(width, width), :])
+            acc[0] + dot(mix_memory[0, :, width:], out_m[pl.ds(width, width), :])
         ).astype(BF16)
 
     for c in range(n_half):
@@ -717,7 +780,7 @@
             pltpu.VMEM((rows, features), BF16),
             pltpu.VMEM((7, features, width), BF16),
             pltpu.VMEM((2 * width, features), BF16),
-            pltpu.VMEM((2 * width, features), BF16),
+            pltpu.VMEM((features // width, 2 * width, width), BF16),
             pltpu.VMEM((rows, width), BF16),
             pltpu.VMEM((rows, width), BF16),
             pltpu.VMEM((rows, width), BF16),
@@ -730,6 +793,7 @@
             pltpu.VMEM((nblocks, PAD, BLOCK), F32),
             pltpu.VMEM((nblocks, PAD, BLOCK), F32),
             pltpu.VMEM((nblocks, heads, dh, dh), BF16),
+            pltpu.VMEM((nblocks, BLOCK, BLOCK), F32),
             pltpu.VMEM((nblocks, BLOCK, BLOCK), F32),
             pltpu.VMEM((2, heads, dh, dh), F32),
             pltpu.VMEM((2, PAD, BLOCK), F32),
@@ -747,16 +811,17 @@
             pltpu.VMEM((heads, RIM, dh), F32),
             pltpu.VMEM((2, half, 2 * width), BF16),
             pltpu.VMEM((2, half, 2 * width), BF16),
-            pltpu.VMEM((half, features), F32),
+            pltpu.VMEM((2, half, features), F32),
             dma((n_half,)),
             dma((9,)),
-            dma((9,)),
+            dma((8 + features // width,)),
             dma((n_half,)),
             dma((n_half,)),
-            dma((2,)),
-            dma((2,)),
+            dma((1 + features // width,)),
+            dma((1 + features // width,)),
             dma((BATCHES + 1,)),
             dma((BATCHES + 1,)),
+            pltpu.SemaphoreType.REGULAR,
             dma((2,)),
             dma((2,)),
             dma((n_half,)),

time: 34.1 us -> 32.8 us (0.962)
  Pallas kernels: 32.3 us -> 31.3 us
    pallas_call x1, Pallas kernels: 32.3 us -> 31.3 us  [local(): pl.pallas_call(functools.partial(kernel, n_sp), name='layer', out_shape=p...]
where the time goes in v3:
time: 32.8 us; the launch traced here: 32.6 us
  Pallas kernels  31.3 us (95%)
  local copies, waits for them, and re-layouts  1.32 us (4%)
    pallas_call x1, Pallas kernels, local(): pl.pallas_call(functools.partial(kernel, n_sp), name='layer', out_shape=p...  31.3 us
    unnamed x1, local copies, waits for them, and re-layouts  1.32 us

profile of v3, /device:TPU:10, one launch (start us, length us, event | category | flops | bytes accessed | tf_op | source)
XLA Modules:
  0.0 32.6 jit_solution(5491788915586388480)
XLA Ops:
  0.0 31.3 %layer.1 = bf16[512,2048]{1,0:T(8,128)(2,1)S(1)} custom-call(bf16[512,2048]{1,0:T(8,128)(2,1)} %bitcast.11, bf16[16,128]{1,0:T(8,128)(2,1)} %bitcast.16, bf16[2048,512]{1,0:T(8,128)(2,1)} %w_key.1, bf16[2048,512]{1,0:T(8,128)(2,1)} %w_value.1, bf16[2048,512]{1,0:T(8,128)(2,1)} %w_query.1, bf16[2048,512]{1,0:T(8,128)(2,1)} %w_gatein.1, ...), custom_call_target="tpu_custom_call" | custom-call | tf_op jit(solution)/shard_map/layer/pallas_call | solution.py:761
  31.3 1.3 %copy.21 = bf16[1,512,2048]{2,1,0:T(8,128)(2,1)} copy(bf16[1,512,2048]{2,1,0:T(8,128)(2,1)S(1)} %bitcast.10) | data formatting | bytes 4194304

commit v4 on v3

--- a/solution.py
+++ b/solution.py
@@ -611,25 +611,23 @@
         conv_sem.at[1],
     )
 
-    @pl.loop(split + 2, n_main)
-    def _(g):
-        relays(g)
-        turn = g - (split + 2)
-        side = jnp.where(turn == 0, other, me)
-        unit(
-            og_rows,
-            OUT_GATE,
-            turn,
-            (),
-            [
-                functools.partial(convolve, side * n_half + j, 1 - turn, j)
-                for j in range(n_half)
-            ],
-        )
-
-        @pl.when(turn == 0)
-        def _():
-            conv_copy.start()
+    relays(split + 2)
+
+    @region
+    def _():
+        for turn, side in enumerate((other, me)):
+            unit(
+                og_rows,
+                OUT_GATE,
+                turn,
+                (),
+                [
+                    functools.partial(convolve, side * n_half + j, 1 - turn, j)
+                    for j in range(n_half)
+                ],
+            )
+            if turn == 0:
+                conv_copy.start()
 
     relays(n_main)
     for c in out_copies:

time: 32.8 us -> 32.9 us (level)
  no operation moved by 1% of the time
where the time goes in v4:
time: 32.9 us; the launch traced here: 32.7 us
  Pallas kernels  31.4 us (95%)
  local copies, waits for them, and re-layouts  1.32 us (4%)
    pallas_call x1, Pallas kernels, local(): pl.pallas_call(functools.partial(kernel, n_sp), name='layer', out_shape=p...  31.4 us
    unnamed x1, local copies, waits for them, and re-layouts  1.32 us

profile of v4, /device:TPU:10, one launch (start us, length us, event | category | flops | bytes accessed | tf_op | source)
XLA Modules:
  0.0 32.7 jit_solution(18297483522552855994)
XLA Ops:
  0.0 31.4 %layer.1 = bf16[512,2048]{1,0:T(8,128)(2,1)S(1)} custom-call(bf16[512,2048]{1,0:T(8,128)(2,1)} %bitcast.11, bf16[16,128]{1,0:T(8,128)(2,1)} %bitcast.16, bf16[2048,512]{1,0:T(8,128)(2,1)} %w_key.1, bf16[2048,512]{1,0:T(8,128)(2,1)} %w_value.1, bf16[2048,512]{1,0:T(8,128)(2,1)} %w_query.1, bf16[2048,512]{1,0:T(8,128)(2,1)} %w_gatein.1, ...), custom_call_target="tpu_custom_call" | custom-call | tf_op jit(solution)/shard_map/layer/pallas_call | solution.py:759
  31.4 1.3 %copy.21 = bf16[1,512,2048]{2,1,0:T(8,128)(2,1)} copy(bf16[1,512,2048]{2,1,0:T(8,128)(2,1)S(1)} %bitcast.10) | data formatting | bytes 4194304
